TPU v7x, 32 devices: a whole 2x2x4 slice. The times are simulated.
32 devices in a mesh: sp: 16 (over z, y, x), tp: 2 (over core).
Axes of the slice: x: 2, y: 2, z: 4, core: 2. Of those that a mesh axis runs over, the one named last changes fastest.
Arguments:
- resid: bfloat16 [3072, 2048], P('sp'), may hold values from -6 to 6
- queries: bfloat16 [3072, 1024], P('sp', 'tp'), may hold values from -6.5 to 6.5
- keys: bfloat16 [3072, 1024], P('sp', 'tp'), may hold values from -6.5 to 6.5
- values: bfloat16 [3072, 1024], P('sp', 'tp'), may hold values from -6 to 6
- lambdas: float32 [8], P('tp'), may hold values from 0.3 to 0.8
- head_gain: float32 [128], replicated, may hold values from 0.1 to 1.9
- out_weight: bfloat16 [1024, 2048], P('tp'), may hold values from -0.1875 to 0.1875
- norm_gain: float32 [2048], replicated, may hold values from 0.1 to 1.9
- gate_weight: bfloat16 [2048, 5632], P('sp', 'tp'), may hold values from -0.125 to 0.125
- up_weight: bfloat16 [2048, 5632], P('sp', 'tp'), may hold values from -0.125 to 0.125
- down_weight: bfloat16 [5632, 2048], P('tp', 'sp'), may hold values from -0.078125 to 0.078125
Outputs:
- result: bfloat16 [3072, 2048], P('sp')
All inputs are finite; a program needn't handle non-finite values.
Results may differ from a plain program's by a relative error of at most 0.014.
Values may be sent and summed in bfloat16 or wider, within the bound.
No kernel may reach another device: no remote copies, remote signals or barrier semaphores. Data moves between devices by JAX's collectives and lax.ppermute only.
A program may use at most 128 MiB of HBM per device.

v0:
```python
import jax
import jax.numpy as jnp
from jax import lax
from jax.sharding import PartitionSpec as P

QK = 64
VD = 128


def rms_rows(first, norm_gain):
    return (
        first * lax.rsqrt(jnp.mean(first * first, axis=-1, keepdims=True) + 1e-06) * norm_gain
    ).astype(jnp.bfloat16)


def local(
    resid,
    queries,
    keys,
    values,
    lambdas,
    head_gain,
    out_weight,
    norm_gain,
    gate_weight,
    up_weight,
    down_weight,
):
    tok_rows = queries.shape[0]
    local_heads = lambdas.shape[0]
    model_width = resid.shape[1]
    offset = lax.axis_index("sp") * tok_rows
    query_four = queries.reshape(tok_rows, local_heads, 2, QK)
    score_scale = QK ** (-0.5)
    query_pos = offset + lax.iota(jnp.int32, tok_rows)
    last_query = offset + tok_rows - 1

    def update(fold_state, key_part, value_part, key_pos):
        run_max, run_sum, run_acc = fold_state
        scores = (
            jnp.einsum("qhcd,khcd->chqk", query_four, key_part, preferred_element_type=jnp.float32)
            * score_scale
        )
        causal_mask = key_pos[None, :] <= query_pos[:, None]
        scores = jnp.where(causal_mask, scores, -1e30)
        new_max = jnp.maximum(run_max, jnp.max(scores, axis=-1))
        expo = jnp.where(causal_mask, jnp.exp(scores - new_max[..., None]), 0.0)
        factor = jnp.exp(run_max - new_max)
        new_sum = run_sum * factor + jnp.sum(expo, axis=-1)
        new_acc = run_acc * factor[..., None] + jnp.einsum(
            "chqk,khd->chqd",
            expo.astype(jnp.bfloat16),
            value_part,
            preferred_element_type=jnp.float32,
        )
        return (new_max, new_sum, new_acc)

    initial = (
        jnp.full((2, local_heads, tok_rows), -1e30, jnp.float32),
        jnp.zeros((2, local_heads, tok_rows), jnp.float32),
        jnp.zeros((2, local_heads, tok_rows, VD), jnp.float32),
    )
    key_rows = lax.all_gather(keys, "sp", axis=0, tiled=True)
    value_rows = lax.all_gather(values, "sp", axis=0, tiled=True)
    key_count = key_rows.shape[0]
    key_span = key_count
    while key_span > 1024 and key_span % 2 == 0:
        key_span = key_span // 2

    def one_span(span_index, inner_state):
        span_start = span_index * key_span
        key_part = lax.dynamic_slice_in_dim(key_rows, span_start, key_span, 0).reshape(
            key_span, local_heads, 2, QK
        )
        value_part = lax.dynamic_slice_in_dim(value_rows, span_start, key_span, 0).reshape(
            key_span, local_heads, VD
        )
        key_pos = span_start + lax.iota(jnp.int32, key_span)
        return update(inner_state, key_part, value_part, key_pos)

    def run_spans(inner_state):
        return lax.fori_loop(0, key_count // key_span, one_span, inner_state)

    def keep_state(inner_state):
        return inner_state

    final_max, final_sum, final_acc = lax.cond(
        jnp.int32(0) <= last_query, run_spans, keep_state, initial
    )
    ratio = final_acc / final_sum[..., None]
    mixed_heads = ratio[0] - lambdas[:, None, None] * ratio[1]
    head_out = (
        mixed_heads
        * lax.rsqrt(jnp.mean(mixed_heads * mixed_heads, axis=-1, keepdims=True) + 1e-05)
        * head_gain
    ).astype(jnp.bfloat16)
    out_three = out_weight.reshape(local_heads, VD, model_width)
    own_count = tok_rows // lax.axis_size("tp")
    branch = lax.psum_scatter(
        jnp.einsum("hqd,hde->qe", head_out, out_three, preferred_element_type=jnp.float32).astype(
            jnp.bfloat16
        ),
        "tp",
        scatter_dimension=0,
        tiled=True,
    ).astype(jnp.float32)
    resid_own = lax.dynamic_slice_in_dim(resid, lax.axis_index("tp") * own_count, own_count, 0)
    first = resid_own.astype(jnp.float32) + branch
    normed_all = lax.all_gather(rms_rows(first, norm_gain), "tp", axis=0, tiled=True)
    gate_act = jnp.dot(
        normed_all,
        lax.all_gather(gate_weight, "sp", axis=0, tiled=True),
        preferred_element_type=jnp.float32,
    )
    up_act = jnp.dot(
        normed_all,
        lax.all_gather(up_weight, "sp", axis=0, tiled=True),
        preferred_element_type=jnp.float32,
    )
    hidden = (jax.nn.silu(gate_act) * up_act).astype(jnp.bfloat16)
    terms = jnp.dot(
        hidden,
        lax.all_gather(down_weight, "sp", axis=1, tiled=True),
        preferred_element_type=jnp.float32,
    )
    mixer = lax.psum_scatter(
        terms.astype(jnp.bfloat16), "tp", scatter_dimension=0, tiled=True
    ).astype(jnp.float32)
    finished = (first + 0.5 * mixer).astype(jnp.bfloat16)
    return lax.all_gather(finished, "tp", axis=0, tiled=True)


def solution(mesh):
    return jax.shard_map(
        local,
        mesh=mesh,
        in_specs=(
            P("sp", None),
            P("sp", "tp"),
            P("sp", "tp"),
            P("sp", "tp"),
            P("tp"),
            P(),
            P("tp", None),
            P(),
            P("sp", "tp"),
            P("sp", "tp"),
            P("tp", "sp"),
        ),
        out_specs=P("sp", None),
        check_vma=False,
    )
```

profile of v0, /device:TPU:0, one launch (start us, length us, event | category | flops | bytes accessed | tf_op | source)
XLA Modules:
  0.0 741.6 jit_solution(319168003058939454)
XLA Ops:
  8.1 72.7 %all-gather.6.cloned.1.call-done = bf16[3072,512]{1,0:T(8,128)(2,1)} async-done(((bf16[192,512]{1,0:T(8,128)(2,1)}), bf16[3072,512]{1,0:T(8,128)(2,1)}) %all-gather.6.cloned.1.call-update) | async-done | bytes 3145744 | tf_op jit(solution)/shard_map/all_gather | solution.py:63
  80.7 69.2 %all-gather.8.cloned.1.call-done = bf16[3072,512]{1,0:T(8,128)(2,1)} async-done(((bf16[192,512]{1,0:T(8,128)(2,1)}), bf16[3072,512]{1,0:T(8,128)(2,1)}) %all-gather.8.cloned.1.call-update) | async-done | bytes 3145744 | tf_op jit(solution)/shard_map/all_gather | solution.py:64
  150.0 78.7 %conditional.1 = (f32[2,4,192]{2,1,0:T(4,128)}, f32[2,4,192,128]{3,2,0,1:T(8,128)}) conditional(s32[]{:T(128)} %convert_element_type.38, () %tuple.27, (bf16[192,512]{1,0:T(8,128)(2,1)}, s32[]{:T(128)}, s32[192]{0:T(256)S(1)}, bf16[3072,512]{1,0:T(8,128)(2,1)}, bf16[3072,512]{1,0:T(8,128)(2,1)}) %tuple.28), branch_computations={%region_0.0_spmd, %region_1.6_spmd} | conditional | flops 464347584 | bytes 25131568 | solution.py:87
  151.1 77.6 %while.17 = (s32[]{:T(128)}, f32[2,4,192]{2,1,0:T(4,128)S(1)}, f32[2,4,192]{2,1,0:T(4,128)}, f32[2,4,192,128]{3,2,0,1:T(8,128)}, s32[192]{0:T(256)S(1)}, /*index...) while((s32[]{:T(128)}, f32[2,4,192]{2,1,0:T(4,128)S(1)}, ...), condition=%wide.region_5.5_spmd.clone, body=%wide.region_2.4_spmd.clone.sunk | while | flops 464347392 | bytes 24343476 | solution.py:82
  151.1 2.4 constant_dynamic-slice_fusion.3
  153.5 2.3 copy.60
  155.9 4.2 fusion.41
  160.2 4.3 fusion.42
  166.3 3.6 fusion.44
  169.9 2.4 constant_dynamic-slice_fusion.3
  172.2 2.3 copy.60
  174.7 4.2 fusion.41
  178.9 4.3 fusion.42
  185.7 3.7 fusion.44
  189.5 2.4 constant_dynamic-slice_fusion.3
  191.8 2.3 copy.60
  194.3 4.2 fusion.41
  198.5 4.3 fusion.42
  205.3 3.7 fusion.44
  209.1 2.4 constant_dynamic-slice_fusion.3
  213.9 4.2 fusion.41
  218.1 4.3 fusion.42
  224.9 3.7 fusion.44
  234.5 5.1 reduce-scatter.3.cloned.1.call-done
  242.0 2.5 all_gather.23
  244.5 140.3 %all-gather.10.cloned.1.call-done = bf16[2048,2816]{1,0:T(8,128)(2,1)} async-done(((bf16[128,2816]{1,0:T(8,128)(2,1)}), bf16[2048,2816]{1,0:T(8,128)(2,1)}) %all-gather.10.cloned.1.call-update) | async-done | bytes 11534352 | tf_op jit(solution)/shard_map/all_gather | solution.py:112
  384.7 8.3 %fusion.22 = f32[192,2816]{1,0:T(8,128)} fusion(bf16[192,2048]{1,0:T(8,128)(2,1)} %all_gather.23, bf16[2048,2816]{1,0:T(8,128)(2,1)} %all-gather.10.cloned.1.call-done), kind=kOutput, calls=%fused_computation.42 | convolution fusion | flops 2214592512 | bytes 14483456 | tf_op jit(solution)/shard_map/dot_general | solution.py:110
  393.1 133.9 %all-gather.12.cloned.1.call-done = bf16[2048,2816]{1,0:T(8,128)(2,1)} async-done(((bf16[128,2816]{1,0:T(8,128)(2,1)}), bf16[2048,2816]{1,0:T(8,128)(2,1)}) %all-gather.12.cloned.1.call-update) | async-done | bytes 11534352 | tf_op jit(solution)/shard_map/all_gather | solution.py:117
  527.0 182.8 %all-gather.14.cloned.1.call-done = bf16[2816,2048]{1,0:T(8,128)(2,1)} async-done(((bf16[2816,128]{1,0:T(8,128)(2,1)}), bf16[2816,2048]{1,0:T(8,128)(2,1)}) %all-gather.14.cloned.1.call-update) | async-done | bytes 11534352 | tf_op jit(solution)/shard_map/all_gather | solution.py:123
  709.8 14.0 %convolution_convert_fusion = bf16[192,2048]{1,0:T(8,128)(2,1)} fusion(bf16[2816,2048]{1,0:T(8,128)(2,1)} %all-gather.14.cloned.1.call-done, bf16[192,2048]{1,0:T(8,128)(2,1)} %all_gather.23, bf16[2048,2816]{1,0:T(8,128)(2,1)} %all-gather.12.cloned.1.call-done, f32[192,2816]{1,0:T(8,128)} %fusion.22), kind=kOutput, calls=%fused_computation.25 | convolution fusion | flops 4432822272 | bytes 26804224 | tf_op jit(solution)/shard_map/dot_general | solution.py:121
  723.8 6.5 reduce-scatter.5.cloned.1.call-done
  731.5 2.4 all_gather.27
  (72 shorter events, 24.9 us)
Async XLA Ops:
  6.5 224.6 %copy-start = (bf16[512,2048]{1,0:T(8,128)(2,1)S(1)}, bf16[512,2048]{1,0:T(8,128)(2,1)}, u32[]{:S(2)}) copy-start(bf16[512,2048]{1,0:T(8,128)(2,1)} %param.21) | copy-start | bytes 6291460
  6.5 74.2 %all-gather.6.cloned.1.call-start = ((), (), s32[]{:S(2)}) async-start(), calls=%async_computation.2 | async-start | bytes 3342336 | tf_op jit(solution)/shard_map/all_gather | solution.py:63
  7.3 142.7 %all-gather.8.cloned.1.call-start = ((), (), s32[]{:S(2)}) async-start(), calls=%async_computation.3 | async-start | bytes 3342336 | tf_op jit(solution)/shard_map/all_gather | solution.py:64
  8.0 231.6 %reduce-scatter.3.cloned.1.call-start = ((), (), s32[]{:S(2)}) async-start(), calls=%async_computation.4 | async-start | bytes 1179648 | tf_op jit(solution)/shard_map/reduce_scatter | solution.py:99
  149.9 80.8 %copy-start.4 = (f32[4]{0:T(128)S(1)}, f32[4]{0:T(128)}, u32[]{:S(2)}) copy-start(f32[4]{0:T(128)} %param.19) | copy-start | bytes 52
  149.9 81.2 %copy-start.5 = (f32[128]{0:T(128)S(1)}, f32[128]{0:T(128)}, u32[]{:S(2)}) copy-start(f32[128]{0:T(128)} %param.20) | copy-start | bytes 1540
  231.1 8.5 %copy-start.2 = (bf16[192,2048]{1,0:T(8,128)(2,1)S(1)}, bf16[192,2048]{1,0:T(8,128)(2,1)}, u32[]{:S(2)}) copy-start(bf16[192,2048]{1,0:T(8,128)(2,1)} %param.15) | copy-start | bytes 2359300
  231.1 9.7 %copy-start.3 = (f32[2048]{0:T(1024)S(1)}, f32[2048]{0:T(1024)}, u32[]{:S(2)}) copy-start(f32[2048]{0:T(1024)} %param.22) | copy-start | bytes 24580
  232.7 152.0 %all-gather.10.cloned.1.call-start = ((), (), s32[]{:S(2)}) async-start(), calls=%async_computation.5 | async-start | bytes 12255232 | tf_op jit(solution)/shard_map/all_gather | solution.py:112
  233.3 293.7 %all-gather.12.cloned.1.call-start = ((), (), s32[]{:S(2)}) async-start(), calls=%async_computation.6 | async-start | bytes 12255232 | tf_op jit(solution)/shard_map/all_gather | solution.py:117
  233.9 475.9 %all-gather.14.cloned.1.call-start = ((), (), s32[]{:S(2)}) async-start(), calls=%async_computation.7 | async-start | bytes 12255232 | tf_op jit(solution)/shard_map/all_gather | solution.py:123
  234.4 495.9 %reduce-scatter.5.cloned.1.call-start = ((), (), s32[]{:S(2)}) async-start(), calls=%async_computation.8 | async-start | bytes 1179648 | tf_op jit(solution)/shard_map/reduce_scatter | solution.py:126
  393.1 337.3 %copy-start.1 = (bf16[96,2048]{1,0:T(8,128)(2,1)S(1)}, bf16[96,2048]{1,0:T(8,128)(2,1)}, u32[]{:S(2)}) copy-start(bf16[96,2048]{1,0:T(8,128)(2,1)} %reduce-scatter.3.cloned.1.call-done) | copy-start | bytes 1179652
Sparse Core Ops, SparseCore 0:
  10.1 70.5 all-gather.5
  83.5 66.3 all-gather.7
  232.8 6.6 reduce-scatter.2
  242.2 142.5 all-gather.9
  387.3 139.5 all-gather.11
  529.5 180.2 all-gather.13
  723.9 6.3 reduce-scatter.4
where the time goes:
time: 743 us; the launch traced here: 742 us
  waiting for transfers between devices  613 us (83%)
  matrix products  55.5 us (7%)
  other arithmetic  27.8 us (4%)
  local copies, waits for them, and re-layouts  26 us (3%)
  between operations  13.6 us (2%)
    all_gather x1, waiting for transfers between devices, local(): lax.all_gather(down_weight, 'sp', axis=1, tiled=True)  183 us
    all_gather x1, waiting for transfers between devices, local(): lax.all_gather(gate_weight, 'sp', axis=0, tiled=True)  140 us
    all_gather x1, waiting for transfers between devices, local(): lax.all_gather(up_weight, 'sp', axis=0, tiled=True)  134 us
    all_gather x1, waiting for transfers between devices, local(): key_rows = lax.all_gather(keys, 'sp', axis=0, tiled=True)  72.7 us
    all_gather x1, waiting for transfers between devices, local(): value_rows = lax.all_gather(values, 'sp', axis=0, tiled=True)  69.2 us
    convert_element_type x4, other arithmetic, update(): expo.astype(jnp.bfloat16)  17.4 us
    dot_general x4, matrix products, update(): jnp.einsum('qhcd,khcd->chqk', query_four, key_part, preferred_element_typ...  16.9 us
  transfers between devices with their start and end apart: 7, of which 7 were waited for; matrix products, arithmetic and copies ran while one was open for 1% of the time, Pallas kernels for 0%

commit v1 on v0

--- a/solution.py
+++ b/solution.py
@@ -1,3 +1,4 @@
+import functools
 import jax
 import jax.numpy as jnp
 from jax import lax
@@ -5,6 +6,13 @@
 
 QK = 64
 VD = 128
+
+
+def things_load(work_x, ndim_at):
+    return jnp.concatenate(lax.all_gather(work_x, "sp"), ndim_at)
+
+
+rest_row_all = functools.partial(things_load, ndim_at=1)
 
 
 def rms_rows(first, norm_gain):
@@ -118,11 +126,7 @@
         preferred_element_type=jnp.float32,
     )
     hidden = (jax.nn.silu(gate_act) * up_act).astype(jnp.bfloat16)
-    terms = jnp.dot(
-        hidden,
-        lax.all_gather(down_weight, "sp", axis=1, tiled=True),
-        preferred_element_type=jnp.float32,
-    )
+    terms = jnp.dot(hidden, rest_row_all(down_weight), preferred_element_type=jnp.float32)
     mixer = lax.psum_scatter(
         terms.astype(jnp.bfloat16), "tp", scatter_dimension=0, tiled=True
     ).astype(jnp.float32)

time: 743 us -> 704 us (0.948)
  waiting for transfers between devices: 613 us -> 558 us
  local copies, waits for them, and re-layouts: 26 us -> 41.1 us
    all_gather x1, waiting for transfers between devices: 183 us -> 140 us  [things_load(): return jnp.concatenate(lax.all_gather(work_x, 'sp'), ndim_at)]
    reshape x0 -> x1, local copies, waits for them, and re-layouts: none -> 15.2 us  [things_load(): return jnp.concatenate(lax.all_gather(work_x, 'sp'), ndim_at)]
    all_gather x1, waiting for transfers between devices: 140 us -> 127 us  [local(): lax.all_gather(gate_weight, 'sp', axis=0, tiled=True)]
  transfers between devices with their start and end apart: 7 -> 7, of which waited for: 7 -> 7; matrix products, arithmetic and copies ran while one was open for 1% -> 4% of each run, Pallas kernels for 0% -> 0%
where the time goes in v1:
time: 704 us; the launch traced here: 703 us
  waiting for transfers between devices  558 us (79%)
  matrix products  56.8 us (8%)
  local copies, waits for them, and re-layouts  41.1 us (6%)
  other arithmetic  27.9 us (4%)
  between operations  13.6 us (2%)
    all_gather x1, waiting for transfers between devices, things_load(): return jnp.concatenate(lax.all_gather(work_x, 'sp'), ndim_at)  140 us
    all_gather x1, waiting for transfers between devices, local(): lax.all_gather(up_weight, 'sp', axis=0, tiled=True)  134 us
    all_gather x1, waiting for transfers between devices, local(): lax.all_gather(gate_weight, 'sp', axis=0, tiled=True)  127 us
    all_gather x1, waiting for transfers between devices, local(): key_rows = lax.all_gather(keys, 'sp', axis=0, tiled=True)  72.7 us
    all_gather x1, waiting for transfers between devices, local(): value_rows = lax.all_gather(values, 'sp', axis=0, tiled=True)  69.2 us
    convert_element_type x4, other arithmetic, update(): expo.astype(jnp.bfloat16)  17.4 us
    dot_general x4, matrix products, update(): jnp.einsum('qhcd,khcd->chqk', query_four, key_part, preferred_element_typ...  16.8 us
    dot_general x1, matrix products, local(): jnp.dot(hidden, rest_row_all(down_weight), preferred_element_type=jnp.flo...  15.6 us
  transfers between devices with their start and end apart: 7, of which 7 were waited for; matrix products, arithmetic and copies ran while one was open for 4% of the time, Pallas kernels for 0%

profile of v1, /device:TPU:0, one launch (start us, length us, event | category | flops | bytes accessed | tf_op | source)
XLA Modules:
  0.0 702.6 jit_solution(13149514545786928006)
XLA Ops:
  8.1 72.7 %all-gather.7.cloned.1.call-done = bf16[3072,512]{1,0:T(8,128)(2,1)} async-done(((bf16[192,512]{1,0:T(8,128)(2,1)}), bf16[3072,512]{1,0:T(8,128)(2,1)}) %all-gather.7.cloned.1.call-update) | async-done | bytes 3145744 | tf_op jit(solution)/shard_map/all_gather | solution.py:71
  80.7 69.2 %all-gather.9.cloned.1.call-done = bf16[3072,512]{1,0:T(8,128)(2,1)} async-done(((bf16[192,512]{1,0:T(8,128)(2,1)}), bf16[3072,512]{1,0:T(8,128)(2,1)}) %all-gather.9.cloned.1.call-update) | async-done | bytes 3145744 | tf_op jit(solution)/shard_map/all_gather | solution.py:72
  150.0 78.7 %conditional.1 = (f32[2,4,192]{2,1,0:T(4,128)}, f32[2,4,192,128]{3,2,0,1:T(8,128)}) conditional(s32[]{:T(128)} %convert_element_type.38, () %tuple.27, (bf16[192,512]{1,0:T(8,128)(2,1)}, s32[]{:T(128)}, s32[192]{0:T(256)S(1)}, bf16[3072,512]{1,0:T(8,128)(2,1)}, bf16[3072,512]{1,0:T(8,128)(2,1)}) %tuple.28), branch_computations={%region_0.0_spmd, %region_1.6_spmd} | conditional | flops 464347584 | bytes 25131568 | solution.py:95
  151.1 77.6 %while.17 = (s32[]{:T(128)}, f32[2,4,192]{2,1,0:T(4,128)S(1)}, f32[2,4,192]{2,1,0:T(4,128)}, f32[2,4,192,128]{3,2,0,1:T(8,128)}, s32[192]{0:T(256)S(1)}, /*index...) while((s32[]{:T(128)}, f32[2,4,192]{2,1,0:T(4,128)S(1)}, ...), condition=%wide.region_5.5_spmd.clone, body=%wide.region_2.4_spmd.clone.sunk | while | flops 464347392 | bytes 24343476 | solution.py:90
  151.1 2.4 constant_dynamic-slice_fusion.3
  153.5 2.3 copy.72
  155.9 4.2 fusion.41
  160.1 4.3 fusion.42
  166.3 3.6 fusion.44
  169.9 2.4 constant_dynamic-slice_fusion.3
  172.2 2.3 copy.72
  174.7 4.2 fusion.41
  178.9 4.3 fusion.42
  185.7 3.7 fusion.44
  189.4 2.4 constant_dynamic-slice_fusion.3
  194.3 4.2 fusion.41
  198.5 4.3 fusion.42
  205.3 3.7 fusion.44
  209.0 2.4 constant_dynamic-slice_fusion.3
  213.8 4.2 fusion.41
  218.1 4.3 fusion.42
  224.9 3.7 fusion.44
  234.5 5.1 reduce-scatter.3.cloned.1.call-done
  241.9 2.5 all_gather.26
  244.5 140.2 %all-gather.15.cloned.1.call-done = bf16[45056,128]{1,0:T(8,128)(2,1)} async-done(((bf16[2816,128]{1,0:T(8,128)(2,1)}), bf16[45056,128]{1,0:T(8,128)(2,1)}) %all-gather.15.cloned.1.call-update) | async-done | bytes 11534352 | tf_op jit(solution)/shard_map/all_gather | solution.py:12
  384.7 15.2 %copy.48 = bf16[2816,16,128]{0,2,1:T(8,128)(2,1)} copy(bf16[2816,16,128]{2,0,1:T(8,128)(2,1)} %bitcast.77) | data formatting | bytes 23068672 | tf_op jit(solution)/shard_map/reshape | solution.py:12
  399.9 127.0 %all-gather.11.cloned.1.call-done = bf16[2048,2816]{1,0:T(8,128)(2,1)} async-done(((bf16[128,2816]{1,0:T(8,128)(2,1)}), bf16[2048,2816]{1,0:T(8,128)(2,1)}) %all-gather.11.cloned.1.call-update) | async-done | bytes 11534352 | tf_op jit(solution)/shard_map/all_gather | solution.py:120
  526.9 8.0 %fusion.22 = f32[192,2816]{1,0:T(8,128)} fusion(bf16[192,2048]{1,0:T(8,128)(2,1)S(1)} %all_gather.26, bf16[2048,2816]{1,0:T(8,128)(2,1)} %all-gather.11.cloned.1.call-done), kind=kOutput, calls=%fused_computation.42 | convolution fusion | flops 2214592512 | bytes 14483456 | tf_op jit(solution)/shard_map/dot_general | solution.py:118
  535.0 134.2 %all-gather.13.cloned.1.call-done = bf16[2048,2816]{1,0:T(8,128)(2,1)} async-done(((bf16[128,2816]{1,0:T(8,128)(2,1)}), bf16[2048,2816]{1,0:T(8,128)(2,1)}) %all-gather.13.cloned.1.call-update) | async-done | bytes 11534352 | tf_op jit(solution)/shard_map/all_gather | solution.py:125
  669.2 15.6 %convolution_convert_fusion = bf16[192,2048]{1,0:T(8,128)(2,1)} fusion(bf16[2816,2048]{0,1:T(8,128)(2,1)} %bitcast.78, bf16[192,2048]{1,0:T(8,128)(2,1)} %copy-done.4, bf16[2048,2816]{1,0:T(8,128)(2,1)} %all-gather.13.cloned.1.call-done, f32[192,2816]{1,0:T(8,128)} %fusion.22), kind=kOutput, calls=%fused_computation.25 | convolution fusion | flops 4432822272 | bytes 26804224 | tf_op jit(solution)/shard_map/dot_general | solution.py:129
  684.8 6.5 reduce-scatter.5.cloned.1.call-done
  692.5 2.4 all_gather.31
  (77 shorter events, 27.2 us)
Async XLA Ops:
  6.5 224.5 %copy-start = (bf16[512,2048]{1,0:T(8,128)(2,1)S(1)}, bf16[512,2048]{1,0:T(8,128)(2,1)}, u32[]{:S(2)}) copy-start(bf16[512,2048]{1,0:T(8,128)(2,1)} %param.21) | copy-start | bytes 6291460
  6.5 74.2 %all-gather.7.cloned.1.call-start = ((), (), s32[]{:S(2)}) async-start(), calls=%async_computation.2 | async-start | bytes 3342336 | tf_op jit(solution)/shard_map/all_gather | solution.py:71
  7.3 142.7 %all-gather.9.cloned.1.call-start = ((), (), s32[]{:S(2)}) async-start(), calls=%async_computation.3 | async-start | bytes 3342336 | tf_op jit(solution)/shard_map/all_gather | solution.py:72
  8.0 231.5 %reduce-scatter.3.cloned.1.call-start = ((), (), s32[]{:S(2)}) async-start(), calls=%async_computation.4 | async-start | bytes 1179648 | tf_op jit(solution)/shard_map/reduce_scatter | solution.py:107
  149.9 80.8 %copy-start.6 = (f32[4]{0:T(128)S(1)}, f32[4]{0:T(128)}, u32[]{:S(2)}) copy-start(f32[4]{0:T(128)} %param.19) | copy-start | bytes 52
  149.9 81.1 %copy-start.7 = (f32[128]{0:T(128)S(1)}, f32[128]{0:T(128)}, u32[]{:S(2)}) copy-start(f32[128]{0:T(128)} %param.20) | copy-start | bytes 1540
  231.1 8.5 %copy-start.3 = (bf16[192,2048]{1,0:T(8,128)(2,1)S(1)}, bf16[192,2048]{1,0:T(8,128)(2,1)}, u32[]{:S(2)}) copy-start(bf16[192,2048]{1,0:T(8,128)(2,1)} %param.15) | copy-start | bytes 2359300
  231.1 9.7 %copy-start.5 = (f32[2048]{0:T(1024)S(1)}, f32[2048]{0:T(1024)}, u32[]{:S(2)}) copy-start(f32[2048]{0:T(1024)} %param.22) | copy-start | bytes 24580
  232.7 152.0 %all-gather.15.cloned.1.call-start = ((), (), s32[]{:S(2)}) async-start(), calls=%async_computation.8 | async-start | bytes 12255232 | tf_op jit(solution)/shard_map/all_gather | solution.py:12
  233.2 293.7 %all-gather.11.cloned.1.call-start = ((), (), s32[]{:S(2)}) async-start(), calls=%async_computation.5 | async-start | bytes 12255232 | tf_op jit(solution)/shard_map/all_gather | solution.py:120
  233.8 435.4 %all-gather.13.cloned.1.call-start = ((), (), s32[]{:S(2)}) async-start(), calls=%async_computation.6 | async-start | bytes 12255232 | tf_op jit(solution)/shard_map/all_gather | solution.py:125
  234.4 456.9 %reduce-scatter.5.cloned.1.call-start = ((), (), s32[]{:S(2)}) async-start(), calls=%async_computation.7 | async-start | bytes 1179648 | tf_op jit(solution)/shard_map/reduce_scatter | solution.py:130
  244.5 282.5 %copy-start.4 = (bf16[192,2048]{1,0:T(8,128)(2,1)}, bf16[192,2048]{1,0:T(8,128)(2,1)S(1)}, u32[]{:S(2)}) copy-start(bf16[192,2048]{1,0:T(8,128)(2,1)S(1)} %all_gather.26) | copy-start | bytes 2359300
  669.2 22.1 %copy-start.2 = (bf16[96,2048]{1,0:T(8,128)(2,1)S(1)}, bf16[96,2048]{1,0:T(8,128)(2,1)}, u32[]{:S(2)}) copy-start(bf16[96,2048]{1,0:T(8,128)(2,1)} %reduce-scatter.3.cloned.1.call-done) | copy-start | bytes 1179652
  669.2 26.5 %copy-start.1 = (bf16[512,2048]{1,0:T(8,128)(2,1)S(1)}, bf16[512,2048]{1,0:T(8,128)(2,1)}, u32[]{:S(2)}) copy-start(bf16[512,2048]{1,0:T(8,128)(2,1)} %param.21) | copy-start | bytes 6291460
Sparse Core Ops, SparseCore 0:
  10.1 70.5 all-gather.6
  83.5 66.3 all-gather.8
  232.8 6.6 reduce-scatter.2
  242.1 142.5 all-gather.14
  387.3 139.5 all-gather.10
  529.5 139.5 all-gather.12
  684.9 6.3 reduce-scatter.4
